TPU v7x, 32 devices: a whole 2x2x4 slice. The times are simulated.
32 devices in a mesh: grp: 2 (over x), ep: 8 (over z, y), tp: 2 (over core).
Axes of the slice: x: 2, y: 2, z: 4, core: 2. Of those that a mesh axis runs over, the one named last changes fastest.
Arguments:
- tokens: bfloat16 [8192, 2048], P(('grp', 'ep', 'tp')), parts along dimension 0, may hold values from -6 to 6
- norm_gain: float32 [2048], replicated, may hold values from 0.1 to 1.9
- routes: int32 [8192, 3], P(('grp', 'ep', 'tp')), parts along dimension 0, may hold values from 0 to 7, all different within a row; in each aligned block of 256 rows (0 to 255, 256 to 511, ...) at most 144 rows name the same one
- gates: float32 [8192, 3], P(('grp', 'ep', 'tp')), parts along dimension 0, may hold values from 0.2 to 1.2
- expert_gate: bfloat16 [8, 2048, 512], P('ep', None, 'tp'), may hold values from -0.125 to 0.125
- expert_up: bfloat16 [8, 2048, 512], P('ep', None, 'tp'), may hold values from -0.125 to 0.125
- expert_down: bfloat16 [8, 512, 2048], P('ep', 'tp'), may hold values from -0.25 to 0.25
- shared_gate: bfloat16 [2048, 512], replicated, may hold values from -0.125 to 0.125
- shared_up: bfloat16 [2048, 512], replicated, may hold values from -0.125 to 0.125
- shared_down: bfloat16 [512, 2048], replicated, may hold values from -0.25 to 0.25
Outputs:
- mixed: bfloat16 [8192, 2048], P(('grp', 'ep', 'tp')), parts along dimension 0
There are 2 independent parts, one for each index of `grp`. A program takes and returns all parts, laid end to end along the dimension named above; an argument that names none is the same for every part. Nothing has to cross between parts.
Inputs may be any that keep to these rules, and one draw needn't show every extreme that they name: `routes`: A row names 3 different experts. Among the rows of one device no expert is named by more than 144 rows, and in every draw some expert is named by exactly 144 rows of some device.
All inputs are finite; a program needn't handle non-finite values.
Results may differ from a plain program's by a relative error of at most 0.01.
Values may be sent and summed in bfloat16 or wider, within the bound.
A program may use at most 128 MiB of HBM per device.

v0:
```python
import jax
import jax.numpy as jnp
from jax import lax
from jax.sharding import PartitionSpec as P


def on_device(
    tokens,
    norm_gain,
    routes,
    gates,
    expert_gate,
    expert_up,
    expert_down,
    shared_gate,
    shared_up,
    shared_down,
):
    token_rows, width = tokens.shape
    top_count = routes.shape[1]
    local_experts = expert_gate.shape[0]
    groups = lax.axis_size("ep")
    experts = local_experts * groups
    capacity = 3 * token_rows * top_count // (2 * experts)
    values = tokens.astype(jnp.float32)
    scaling = lax.rsqrt(jnp.mean(values * values, axis=1, keepdims=True) + 1e-06)
    normed = (values * scaling * norm_gain[None, :]).astype(jnp.bfloat16)
    flat_routes = routes.reshape(-1)
    copies = flat_routes.shape[0]
    onehot = (flat_routes[:, None] == jnp.arange(experts, dtype=jnp.int32)[None, :]).astype(
        jnp.int32
    )
    earlier = jnp.cumsum(onehot, axis=0) - onehot
    slot_index = jnp.sum(earlier * onehot, axis=1)
    buffer_row = flat_routes * capacity + slot_index
    source_token = jnp.arange(copies, dtype=jnp.int32) // top_count
    slot_token = (
        jnp.full((experts * capacity,), token_rows, jnp.int32).at[buffer_row].set(source_token)
    )
    padded = jnp.concatenate([normed, jnp.zeros((1, width), jnp.bfloat16)], axis=0)
    outgoing = padded[slot_token].reshape(groups, local_experts, capacity, width)
    whole_gate, whole_up = (
        lax.all_gather(expert_gate, "tp", axis=2, tiled=True),
        lax.all_gather(expert_up, "tp", axis=2, tiled=True),
    )
    whole_down = lax.all_gather(expert_down, "tp", axis=1, tiled=True)
    received = lax.all_to_all(outgoing, "ep", split_axis=0, concat_axis=0, tiled=True)
    gate_values = jnp.einsum(
        "secd,edf->secf", received, whole_gate, preferred_element_type=jnp.float32
    )
    up_values = jnp.einsum("secd,edf->secf", received, whole_up, preferred_element_type=jnp.float32)
    hidden = (jax.nn.silu(gate_values) * up_values).astype(jnp.bfloat16)
    summed = jnp.einsum("secf,efd->secd", hidden, whole_down, preferred_element_type=jnp.float32)
    returned = lax.all_to_all(
        summed.astype(jnp.bfloat16), "ep", split_axis=0, concat_axis=0, tiled=True
    )
    shared_hidden = (
        jax.nn.silu(jnp.dot(normed, shared_gate, preferred_element_type=jnp.float32))
        * jnp.dot(normed, shared_up, preferred_element_type=jnp.float32)
    ).astype(jnp.bfloat16)
    shared_out = jnp.dot(shared_hidden, shared_down, preferred_element_type=jnp.float32)
    flat_back = returned.reshape(experts * capacity, width)
    picked = flat_back[buffer_row].reshape(token_rows, top_count, width)
    routed = jnp.einsum("tkd,tk->td", picked.astype(jnp.float32), gates)
    return (shared_out + routed).astype(jnp.bfloat16)


def solution(mesh):
    return jax.shard_map(
        on_device,
        mesh=mesh,
        in_specs=(
            P(("grp", "ep", "tp"), None),
            P(),
            P(("grp", "ep", "tp"), None),
            P(("grp", "ep", "tp"), None),
            P("ep", None, "tp"),
            P("ep", None, "tp"),
            P("ep", "tp", None),
            P(),
            P(),
            P(),
        ),
        out_specs=P(("grp", "ep", "tp"), None),
        check_vma=False,
    )
```

profile of v0, /device:TPU:0, one launch (start us, length us, event | category | flops | bytes accessed | tf_op | source)
XLA Modules:
  0.0 299.9 jit_solution(8163634052735282706)
XLA Ops:
  6.5 1.0 copy.19
  7.9 0.7 broadcast_multiply_fusion
  8.6 1.7 reduce-window.6
  11.0 0.2 mul.61
  11.3 3.4 %scatter_custom_fusion = s32[1152]{0:T(1024)S(1)} fusion(s32[768]{0:T(1024)S(1)} %fusion.43, s32[768]{0:T(1024)S(1)} %add_select_fusion, s32[]{:T(128)} %constant.18.clone.1), kind=kCustom, calls=%fused_computation.50 | custom fusion | bytes 4612 | tf_op jit(solution)/shard_map/scatter | solution.py:38
  14.7 1.5 fusion.9
  16.2 1.0 fusion.11
  17.3 1.0 copy-done.2
  18.3 6.0 %gather_fusion = bf16[1152,2048]{1,0:T(8,128)(2,1)} fusion(bf16[257,2048]{1,0:T(8,128)(2,1)S(1)} %concatenate.3, s32[2048]{0:T(1024)S(1)} %pad_clamp_fusion), kind=kCustom, calls=%fused_computation | custom fusion | bytes 9441792 | tf_op jit(solution)/shard_map/gather | solution.py:41
  24.3 7.3 %all-to-all-start = ((bf16[8,1,144,2048]{3,2,1,0:T(8,128)(2,1)}), bf16[8,1,144,2048]{3,2,1,0:T(8,128)(2,1)}, u32[]{:S(2)}, u32[]{:S(2)}) async-start(bf16[8,1,144,2048]{3,2,1,0:T(8,128)(2,1)} %bitcast.98), calls=%async_computation | async-start | bytes 9437184 | tf_op jit(solution)/shard_map/all_to_all | solution.py:47
  31.7 0.7 all-gather.6.cloned.1.call-update
  32.4 0.7 all-gather.4.cloned.1.call-update
  33.1 0.7 all-gather.8.cloned.1.call-update
  33.8 11.7 %all-gather.6.cloned.1.call-done = bf16[1,2048,512]{2,1,0:T(8,128)(2,1)} async-done(((bf16[1,2048,256]{2,1,0:T(8,128)(2,1)}), bf16[1,2048,512]{2,1,0:T(8,128)(2,1)}) %all-gather.6.cloned.1.call-update) | async-done | bytes 2097168 | tf_op jit(solution)/shard_map/all_gather | solution.py:44
  45.5 90.6 %all-to-all-done = bf16[8,1,144,2048]{3,2,1,0:T(8,128)(2,1)} async-done(((bf16[8,1,144,2048]{3,2,1,0:T(8,128)(2,1)}), bf16[8,1,144,2048]{3,2,1,0:T(8,128)(2,1)}, u32[]{:S(2)}, u32[]{:S(2)}) %all-to-all-start) | async-done | bytes 4718624 | tf_op jit(solution)/shard_map/all_to_all | solution.py:47
  136.1 7.0 %fusion = f32[8,144,512]{2,1,0:T(8,128)} fusion(bf16[8,1,144,2048]{3,2,1,0:T(8,128)(2,1)} %all-to-all-done, bf16[1,2048,512]{2,1,0:T(8,128)(2,1)} %all-gather.6.cloned.1.call-done), kind=kOutput, calls=%fused_computation.3 | convolution fusion | flops 2415919104 | bytes 9175040 | tf_op jit(solution)/shard_map/secd,edf->secf/dot_general | solution.py:51
  143.2 11.7 %convert_bitcast_fusion = bf16[8,1,144,2048]{3,2,1,0:T(8,128)(2,1)} fusion(bf16[1,512,2048]{2,1,0:T(8,128)(2,1)} %all-gather.8.cloned.1.call-done, f32[8,144,512]{2,1,0:T(8,128)} %fusion, bf16[1,2048,512]{2,1,0:T(8,128)(2,1)} %all-gather.4.cloned.1.call-done, bf16[8,1,144,2048]{3,2,1,0:T(8,128)(2,1)} %all-to-all-done), kind=kOutput, calls=%fused_computation.7 | convolution fusion | flops 4837736448 | bytes 15990784 | tf_op jit(solution)/shard_map/secf,efd->secd/dot_general | solution.py:53
  154.9 4.9 %all-to-all-start.1 = ((bf16[8,1,144,2048]{3,2,1,0:T(8,128)(2,1)}), bf16[8,1,144,2048]{3,2,1,0:T(8,128)(2,1)}, u32[]{:S(2)}, u32[]{:S(2)}) async-start(bf16[8,1,144,2048]{3,2,1,0:T(8,128)(2,1)} %convert_bitcast_fusion), calls=%async_computation.1 | async-start | bytes 9437184 | tf_op jit(solution)/shard_map/all_to_all | solution.py:54
  160.0 3.1 %fusion.46 = f32[256,512]{1,0:T(8,128)} fusion(bf16[256,2048]{1,0:T(8,128)(2,1)S(1)} %copy-done.3, bf16[2048,512]{1,0:T(8,128)(2,1)} %param.17), kind=kOutput, calls=%fused_computation.58 | convolution fusion | flops 536870912 | bytes 3670016 | tf_op jit(solution)/shard_map/dot_general | solution.py:58
  163.1 100.3 %all-to-all-done.1 = bf16[8,1,144,2048]{3,2,1,0:T(8,128)(2,1)} async-done(((bf16[8,1,144,2048]{3,2,1,0:T(8,128)(2,1)}), bf16[8,1,144,2048]{3,2,1,0:T(8,128)(2,1)}, u32[]{:S(2)}, u32[]{:S(2)}) %all-to-all-start.1) | async-done | bytes 4718624 | tf_op jit(solution)/shard_map/all_to_all | solution.py:54
  263.4 10.0 %gather_fusion.1 = bf16[768,2048]{1,0:T(8,128)(2,1)} fusion(bf16[1152,2048]{1,0:T(8,128)(2,1)} %bitcast.25, s32[1024]{0:T(1024)S(1)} %pad_clamp_fusion.1), kind=kCustom, calls=%fused_computation.1 | custom fusion | bytes 6294528 | tf_op jit(solution)/shard_map/gather | solution.py:63
  273.4 9.1 %reshape.92 = bf16[256,3,2048]{2,1,0:T(4,128)(2,1)} reshape(bf16[768,2048]{1,0:T(8,128)(2,1)} %gather_fusion.1) | data formatting | bytes 6291456 | tf_op jit(solution)/shard_map/reshape | solution.py:63
  282.5 5.8 %fusion.47 = f32[256,1,2048]{2,1,0:T(1,128)} fusion(bf16[256,3,2048]{2,1,0:T(4,128)(2,1)} %reshape.92, bf16[256,3,1]{1,2,0:T(2,128)(2,1)S(1)} %copy.25), kind=kOutput, calls=%fused_computation.59 | convolution fusion | flops 3145728 | bytes 5244416 | tf_op jit(solution)/shard_map/tkd,tk->td/dot_general | solution.py:64
  288.3 5.1 %fusion.4 = bf16[256,2048]{1,0:T(8,128)(2,1)} fusion(bf16[512,2048]{1,0:T(8,128)(2,1)S(1)} %copy-done, f32[256,1,2048]{2,1,0:T(1,128)} %fusion.47, bf16[256,2048]{1,0:T(8,128)(2,1)S(1)} %copy-done.3, bf16[2048,512]{1,0:T(8,128)(2,1)} %param.18, f32[256,512]{1,0:T(8,128)} %fusion.46), kind=kOutput, calls=%fused_computation.11 | convolution fusion | flops 1075576832 | bytes 8912896 | tf_op jit(solution)/shard_map/dot_general | solution.py:61
  (31 shorter events, 1.5 us)
Async XLA Ops:
  6.5 281.8 %copy-start = (bf16[512,2048]{1,0:T(8,128)(2,1)S(1)}, bf16[512,2048]{1,0:T(8,128)(2,1)}, u32[]{:S(2)}) copy-start(bf16[512,2048]{1,0:T(8,128)(2,1)} %param.19) | copy-start | bytes 6291460
  6.5 9.7 %copy-start.1 = (bf16[256,2048]{1,0:T(8,128)(2,1)S(1)}, bf16[256,2048]{1,0:T(8,128)(2,1)}, u32[]{:S(2)}) copy-start(bf16[256,2048]{1,0:T(8,128)(2,1)} %param.10) | copy-start | bytes 3145732
  17.2 1.0 copy-start.2
  24.3 111.8 %all-to-all-start = ((bf16[8,1,144,2048]{3,2,1,0:T(8,128)(2,1)}), bf16[8,1,144,2048]{3,2,1,0:T(8,128)(2,1)}, u32[]{:S(2)}, u32[]{:S(2)}) async-start(bf16[8,1,144,2048]{3,2,1,0:T(8,128)(2,1)} %bitcast.98), calls=%async_computation | async-start | bytes 9437184 | tf_op jit(solution)/shard_map/all_to_all | solution.py:47
  31.6 13.9 %all-gather.6.cloned.1.call-start = ((), (), s32[]{:S(2)}) async-start(), calls=%async_computation.3 | async-start | bytes 3145728 | tf_op jit(solution)/shard_map/all_gather | solution.py:44
  32.3 110.8 %all-gather.4.cloned.1.call-start = ((), (), s32[]{:S(2)}) async-start(), calls=%async_computation.2 | async-start | bytes 3145728 | tf_op jit(solution)/shard_map/all_gather | solution.py:43
  33.1 110.1 %all-gather.8.cloned.1.call-start = ((), (), s32[]{:S(2)}) async-start(), calls=%async_computation.4 | async-start | bytes 3145728 | tf_op jit(solution)/shard_map/all_gather | solution.py:46
  154.9 4.9 %copy-start.4 = (f32[256,3]{0,1:T(4,128)S(1)}, f32[256,3]{0,1:T(4,128)}, u32[]{:S(2)}) copy-start(f32[256,3]{0,1:T(4,128)} %param.13) | copy-start | bytes 9220
  154.9 5.1 %copy-start.3 = (bf16[256,2048]{1,0:T(8,128)(2,1)S(1)}, bf16[256,2048]{1,0:T(8,128)(2,1)}, u32[]{:S(2)}) copy-start(bf16[256,2048]{1,0:T(8,128)(2,1)} %copy-done.2) | copy-start | bytes 3145732
  154.9 108.5 %all-to-all-start.1 = ((bf16[8,1,144,2048]{3,2,1,0:T(8,128)(2,1)}), bf16[8,1,144,2048]{3,2,1,0:T(8,128)(2,1)}, u32[]{:S(2)}, u32[]{:S(2)}) async-start(bf16[8,1,144,2048]{3,2,1,0:T(8,128)(2,1)} %convert_bitcast_fusion), calls=%async_computation.1 | async-start | bytes 9437184 | tf_op jit(solution)/shard_map/all_to_all | solution.py:54
Sparse Core Ops, SparseCore 0:
  34.0 11.4 all-gather.5
  47.0 11.2 all-gather.3
  59.9 11.7 all-gather.7
where the time goes:
time: 301 us; the launch traced here: 300 us
  waiting for transfers between devices  205 us (68%)
  matrix products  32.7 us (11%)
  local copies, waits for them, and re-layouts  31.7 us (11%)
  between operations  13.3 us (4%)
  starting transfers between devices  12.3 us (4%)
  other arithmetic  5.22 us (2%)
    all_to_all x1, waiting for transfers between devices, on_device(): lax.all_to_all(summed.astype(jnp.bfloat16), 'ep', split_axis=0, concat_ax...  100 us
    all_to_all x1, waiting for transfers between devices, on_device(): lax.all_to_all(outgoing, 'ep', split_axis=0, concat_axis=0, tiled=True)  90.6 us
    dot_general x1, matrix products, on_device(): jnp.einsum('secf,efd->secd', hidden, whole_down, preferred_element_type=j...  11.7 us
    all_gather x1, waiting for transfers between devices, on_device(): lax.all_gather(expert_up, 'tp', axis=2, tiled=True)  11.7 us
    gather x1, local copies, waits for them, and re-layouts, on_device(): picked = flat_back[buffer_row].reshape(token_rows, top_count, width)  10 us
    reshape x1, local copies, waits for them, and re-layouts, on_device(): picked = flat_back[buffer_row].reshape(token_rows, top_count, width)  9.09 us
    all_to_all x1, starting transfers between devices, on_device(): lax.all_to_all(outgoing, 'ep', split_axis=0, concat_axis=0, tiled=True)  7.31 us
    dot_general x1, matrix products, on_device(): jnp.einsum('secd,edf->secf', received, whole_up, preferred_element_type=j...  7.04 us
  transfers between devices with their start and end apart: 5, of which 3 were waited for; matrix products, arithmetic and copies ran while one was open for 3% of the time, Pallas kernels for 0%

commit v1 on v0

--- a/solution.py
+++ b/solution.py
@@ -1,10 +1,433 @@
+import functools
+
 import jax
 import jax.numpy as jnp
 from jax import lax
+from jax.experimental import pallas as pl
+from jax.experimental.pallas import tpu as pltpu
 from jax.sharding import PartitionSpec as P
 
-
-def on_device(
+MESH = pl.DeviceIdType.MESH
+
+
+def exchange_kernel(
+    line,
+    tok,
+    gain,
+    wcol,
+    eg,
+    eu,
+    ed,
+    sg,
+    su,
+    sd,
+    out,
+    gathered,
+    G,
+    U,
+    D,
+    SG,
+    SU,
+    SD,
+    xn,
+    hid,
+    acc,
+    stage,
+    land,
+    loc_sem,
+    ag_send,
+    ag_recv,
+    w_send,
+    w_recv,
+    rs_send,
+    rs_recv,
+):
+    rows, width = tok.shape
+    half = eg.shape[1]
+    shared_width = sg.shape[1]
+    last = line - 1
+    ep = lax.axis_index("ep")
+    z, y = ep // 2, ep % 2
+    c = lax.axis_index("tp")
+    g = lax.axis_index("grp")
+    to_next, to_prev = {"ep": ep + 2}, {"ep": ep - 2}
+    to_pair = {"ep": z * 2 + (1 - y)}
+    to_core = {"tp": 1 - c}
+    to_grp = {"grp": 1 - g}
+
+    barrier = pltpu.get_barrier_semaphore()
+    for peer in (to_pair, to_core, to_grp):
+        pl.semaphore_signal(barrier, inc=1, device_id=peer, device_id_type=MESH)
+
+    @pl.when(z < last)
+    def _():
+        pl.semaphore_signal(barrier, inc=1, device_id=to_next, device_id_type=MESH)
+
+    @pl.when(z > 0)
+    def _():
+        pl.semaphore_signal(barrier, inc=1, device_id=to_prev, device_id_type=MESH)
+
+    locals_ = [
+        pltpu.make_async_copy(tok, gathered.at[z], loc_sem.at[0]),
+        pltpu.make_async_copy(sg, SG, loc_sem.at[1]),
+        pltpu.make_async_copy(su, SU, loc_sem.at[2]),
+        pltpu.make_async_copy(sd, SD, loc_sem.at[3]),
+        pltpu.make_async_copy(eg, G.at[0], loc_sem.at[4]),
+        pltpu.make_async_copy(eu, U.at[0], loc_sem.at[5]),
+        pltpu.make_async_copy(ed, D.at[pl.ds(0, half)], loc_sem.at[6]),
+    ]
+    for copy in locals_:
+        copy.start()
+    between = jnp.logical_and(z > 0, z < last)
+
+    @pl.when(between)
+    def _():
+        pl.semaphore_wait(barrier, 5)
+
+    @pl.when(jnp.logical_not(between))
+    def _():
+        pl.semaphore_wait(barrier, 4)
+
+    def remote(src, dst, send, recv, peer):
+        return pltpu.make_async_remote_copy(
+            src_ref=src,
+            dst_ref=dst,
+            send_sem=send,
+            recv_sem=recv,
+            device_id=peer,
+            device_id_type=MESH,
+        )
+
+    def ag_copy(way, step):
+        block = z - step if way == 0 else z + step
+        src = tok if step == 0 else gathered.at[block]
+        peer = to_next if way == 0 else to_prev
+        return remote(
+            src, gathered.at[block], ag_send.at[way, step], ag_recv.at[way, step], peer
+        )
+
+    def ag_sends(way, step):
+        if way == 0:
+            return jnp.logical_and(z - step >= 0, z < last)
+        return jnp.logical_and(z + step <= last, z > 0)
+
+    def ag_arrival(way, step):
+        block = z - 1 - step if way == 0 else z + 1 + step
+        slot = gathered.at[block]
+        peer = to_next if way == 0 else to_prev
+        return remote(slot, slot, ag_send.at[way, step], ag_recv.at[way, step], peer)
+
+    def ag_arrives(way, step):
+        return z - 1 - step >= 0 if way == 0 else z + 1 + step <= last
+
+    def ag_start(step):
+        for way in range(2):
+
+            @pl.when(ag_sends(way, step))
+            def _():
+                ag_copy(way, step).start()
+
+    def ag_wait(step):
+        for way in range(2):
+
+            @pl.when(ag_arrives(way, step))
+            def _():
+                ag_arrival(way, step).wait_recv()
+
+    def piece(k, unit, part):
+        if k == 2:
+            if part is None:
+                return D.at[pl.ds(unit * half, half)]
+            n = half // 2
+            return D.at[pl.ds(pl.multiple_of(unit * half + part * n, n), n)]
+        whole = (G, U)[k].at[unit]
+        if part is None:
+            return whole
+        n = width // 2
+        return whole.at[pl.ds(pl.multiple_of(part * n, n), n)]
+
+    own = (eg, eu, ed)
+
+    def own_part(k):
+        n = own[k].shape[0] // 2
+        return own[k].at[pl.ds(pl.multiple_of(g * n, n), n)]
+
+    def w_copy(kind, k):
+        sems = (w_send.at[kind, k], w_recv.at[kind, k])
+        if kind == 0:
+            return remote(own[k], piece(k, 1, None), *sems, to_core)
+        if kind == 1:
+            return remote(own_part(k), piece(k, 2, g), *sems, to_pair)
+        if kind == 2:
+            return remote(piece(k, 2, g), piece(k, 2, g), *sems, to_grp)
+        if kind == 3:
+            return remote(piece(k, 2, g), piece(k, 3, g), *sems, to_core)
+        return remote(piece(k, 2, 1 - g), piece(k, 3, 1 - g), *sems, to_core)
+
+    def w_arrival(kind, k):
+        if kind != 2:
+            return w_copy(kind, k)
+        slot = piece(k, 2, 1 - g)
+        return remote(slot, slot, w_send.at[kind, k], w_recv.at[kind, k], to_grp)
+
+    ag_start(0)
+    for k in range(3):
+        w_copy(1, k).start()
+    for k in range(3):
+        w_copy(0, k).start()
+
+    tile = 32
+
+    def normalise(block):
+        @pl.loop(0, rows // tile)
+        def _(i):
+            part = pl.ds(pl.multiple_of(i * tile, tile), tile)
+            values = gathered[block, part, :].astype(jnp.float32)
+            scaling = lax.rsqrt(jnp.mean(values * values, axis=1, keepdims=True) + 1e-06)
+            xn[part, :] = (values * scaling * gain[...]).astype(jnp.bfloat16)
+
+    def act(a, b):
+        return a / (1.0 + jnp.exp(-a)) * b
+
+    cols_n = 512 if width % 512 == 0 else width
+
+    def over_columns(fn):
+        @pl.loop(0, width // cols_n)
+        def _(i):
+            fn(pl.ds(pl.multiple_of(i * cols_n, cols_n), cols_n))
+
+    def routed(block, fn):
+        normalise(block)
+
+        @pl.loop(0, 4)
+        def _(u):
+            a = jnp.dot(xn[...], G[u], preferred_element_type=jnp.float32)
+            b = jnp.dot(xn[...], U[u], preferred_element_type=jnp.float32)
+            w = jnp.where(u < 2, wcol[block, :, 0:1], wcol[block, :, 1:2])
+            hid[:, pl.ds(pl.multiple_of(u * half, half), half)] = (act(a, b) * w).astype(
+                jnp.bfloat16
+            )
+
+        over_columns(
+            lambda cols: fn(
+                cols,
+                jnp.dot(
+                    hid[:, 0 : 4 * half], D[:, cols], preferred_element_type=jnp.float32
+                ),
+            )
+        )
+
+    locals_[0].wait()
+    normalise(z)
+    for copy in locals_[1:4]:
+        copy.wait()
+
+    @pl.loop(0, shared_width // half)
+    def _(u):
+        part = pl.ds(pl.multiple_of(u * half, half), half)
+        a = jnp.dot(xn[...], SG[:, part], preferred_element_type=jnp.float32)
+        b = jnp.dot(xn[...], SU[:, part], preferred_element_type=jnp.float32)
+        hid[:, part] = act(a, b).astype(jnp.bfloat16)
+
+    def shared_store(cols):
+        acc[:, cols] = jnp.dot(
+            hid[:, 0:shared_width], SD[:, cols], preferred_element_type=jnp.float32
+        )
+
+    over_columns(shared_store)
+
+    def pass_on(k):
+        w_arrival(1, k).wait_recv()
+        w_copy(2, k).start()
+        w_copy(3, k).start()
+
+    def pass_over(k):
+        w_arrival(2, k).wait_recv()
+        w_copy(4, k).start()
+
+    pass_on(0)
+    pass_on(1)
+    ag_wait(0)
+    if last > 1:
+        ag_start(1)
+    pass_over(0)
+    pass_on(2)
+    pass_over(1)
+    pass_over(2)
+    for copy in locals_[4:]:
+        copy.wait()
+    for kind in (0, 3, 4):
+        for k in range(3):
+            w_arrival(kind, k).wait_recv()
+
+    def add_own(cols, value):
+        acc[:, cols] += value
+
+    routed(z, add_own)
+
+    def rs_sends(way, t):
+        return jnp.logical_and(z <= t, z < last) if way == 0 else jnp.logical_and(
+            last - z <= t, z > 0
+        )
+
+    def partial(t):
+        for way in range(2):
+
+            @pl.when(rs_sends(way, t))
+            def _():
+                block = last - t + z if way == 0 else z - last + t
+
+                def store(cols, value):
+                    stage[way, t, :, cols] = value.astype(jnp.bfloat16)
+
+                routed(block, store)
+
+    def rs_copy(way, t):
+        peer = to_next if way == 0 else to_prev
+        return remote(
+            stage.at[way, t], land.at[way, t], rs_send.at[way, t], rs_recv.at[way, t], peer
+        )
+
+    def over_rows(fn):
+        @pl.loop(0, rows // tile)
+        def _(i):
+            fn(pl.ds(pl.multiple_of(i * tile, tile), tile))
+
+    for t in reversed(range(last)):
+        step = last - 1 - t
+        if step > 0:
+            ag_wait(step)
+            if step + 1 < last:
+                ag_start(step + 1)
+        partial(t)
+
+    for t in range(last):
+        for way in range(2):
+
+            @pl.when(rs_sends(way, t))
+            def _():
+                if t > 0:
+                    inner = z > 0 if way == 0 else z < last
+
+                    @pl.when(inner)
+                    def _():
+                        rs_copy(way, t - 1).wait_recv()
+
+                        def add(part):
+                            stage[way, t, part, :] = (
+                                stage[way, t, part, :].astype(jnp.float32)
+                                + land[way, t - 1, part, :].astype(jnp.float32)
+                            ).astype(jnp.bfloat16)
+
+                        over_rows(add)
+
+                rs_copy(way, t).start()
+
+    for way in range(2):
+
+        @pl.when(z > 0 if way == 0 else z < last)
+        def _():
+            rs_copy(way, last - 1).wait_recv()
+
+            def add(part):
+                acc[part, :] += land[way, last - 1, part, :].astype(jnp.float32)
+
+            over_rows(add)
+
+    def finish(part):
+        out[part, :] = acc[part, :].astype(jnp.bfloat16)
+
+    over_rows(finish)
+
+    for kind in range(5):
+        for k in range(3):
+            w_copy(kind, k).wait_send()
+    for step in range(last):
+        for way in range(2):
+
+            @pl.when(ag_sends(way, step))
+            def _():
+                ag_copy(way, step).wait_send()
+
+            @pl.when(rs_sends(way, step))
+            def _():
+                rs_copy(way, step).wait_send()
+
+
+def gathered_plan(
+    tokens,
+    norm_gain,
+    routes,
+    gates,
+    expert_gate,
+    expert_up,
+    expert_down,
+    shared_gate,
+    shared_up,
+    shared_down,
+):
+    rows, width = tokens.shape
+    groups = lax.axis_size("ep")
+    line = groups // 2
+    half = expert_gate.shape[2]
+    shared_width = shared_gate.shape[1]
+    ep = lax.axis_index("ep")
+    own = jnp.arange(groups, dtype=jnp.int32)
+    weights = jnp.sum(
+        jnp.where(routes[:, :, None] == own[None, None, :], gates[:, :, None], 0.0), axis=1
+    )
+    everyone = lax.all_gather(weights.T, "ep").reshape(line, 2, groups, rows)
+    mine = lax.dynamic_index_in_dim(everyone, ep % 2, 1, keepdims=False)
+    first = lax.dynamic_index_in_dim(mine, ep, 1, keepdims=False)
+    second = lax.dynamic_index_in_dim(mine, ep // 2 * 2 + 1 - ep % 2, 1, keepdims=False)
+    wcol = jnp.stack([first, second], axis=2)
+    any_spec = pl.BlockSpec(memory_space=pl.ANY)
+    vmem_spec = pl.BlockSpec(memory_space=pltpu.VMEM)
+    bf16 = jnp.bfloat16
+    steps = line - 1
+    return pl.pallas_call(
+        functools.partial(exchange_kernel, line),
+        out_shape=jax.ShapeDtypeStruct((rows, width), bf16),
+        in_specs=[any_spec, vmem_spec, vmem_spec] + [any_spec] * 6,
+        out_specs=vmem_spec,
+        scratch_shapes=[
+            pltpu.VMEM((line, rows, width), bf16),
+            pltpu.VMEM((4, width, half), bf16),
+            pltpu.VMEM((4, width, half), bf16),
+            pltpu.VMEM((4 * half, width), bf16),
+            pltpu.VMEM((width, shared_width), bf16),
+            pltpu.VMEM((width, shared_width), bf16),
+            pltpu.VMEM((shared_width, width), bf16),
+            pltpu.VMEM((rows, width), bf16),
+            pltpu.VMEM((rows, max(4 * half, shared_width)), bf16),
+            pltpu.VMEM((rows, width), jnp.float32),
+            pltpu.VMEM((2, steps, rows, width), bf16),
+            pltpu.VMEM((2, steps, rows, width), bf16),
+            pltpu.SemaphoreType.DMA((7,)),
+            pltpu.SemaphoreType.DMA((2, steps)),
+            pltpu.SemaphoreType.DMA((2, steps)),
+            pltpu.SemaphoreType.DMA((5, 3)),
+            pltpu.SemaphoreType.DMA((5, 3)),
+            pltpu.SemaphoreType.DMA((2, steps)),
+            pltpu.SemaphoreType.DMA((2, steps)),
+        ],
+        compiler_params=pltpu.CompilerParams(
+            collective_id=0, has_side_effects=True, vmem_limit_bytes=56 * 1024 * 1024
+        ),
+    )(
+        tokens,
+        norm_gain.reshape(1, width),
+        wcol,
+        expert_gate[0],
+        expert_up[0],
+        expert_down[0],
+        shared_gate,
+        shared_up,
+        shared_down,
+    )
+
+
+def routed_plan(
     tokens,
     norm_gain,
     routes,
@@ -65,6 +488,14 @@
     return (shared_out + routed).astype(jnp.bfloat16)
 
 
+def on_device(*args):
+    experts = args[4].shape[0] * lax.axis_size("ep")
+    paired = lax.axis_size("grp") == 2 and lax.axis_size("tp") == 2
+    if paired and args[4].shape[0] == 1 and experts % 2 == 0 and experts <= 4 * args[2].shape[1]:
+        return gathered_plan(*args)
+    return routed_plan(*args)
+
+
 def solution(mesh):
     return jax.shard_map(
         on_device,

time: 301 us -> 209 us (0.69)
  waiting for transfers between devices: 205 us -> 0 us
  Pallas kernels: 0 us -> 173 us
  matrix products: 32.7 us -> 0 us
  blocking collectives: 0 us -> 32.3 us
  local copies, waits for them, and re-layouts: 31.7 us -> 3.35 us
  between operations: 13.3 us -> 0.03 us
  starting transfers between devices: 12.3 us -> 0 us
  other arithmetic: 5.22 us -> 0.72 us
    all_to_all x2 -> x0, waiting for transfers between devices: 191 us -> none  [the longest x1 100 us: on_device(): lax.all_to_all(summed.astype(jnp.bfloat16), 'ep', split_axis=0, concat_ax...]
    pallas_call x0 -> x1, Pallas kernels: none -> 173 us  [gathered_plan(): pl.pallas_call(functools.partial(exchange_kernel, line), out_shape=jax.Sh...]
    dot_general x5 -> x0, matrix products: 32.7 us -> none  [the longest x1 11.7 us: on_device(): jnp.einsum('secf,efd->secd', hidden, whole_down, preferred_element_type=j...]
    all_gather x0 -> x1, blocking collectives: none -> 32.3 us  [gathered_plan(): everyone = lax.all_gather(weights.T, 'ep').reshape(line, 2, groups, rows)]
    gather x2 -> x0, local copies, waits for them, and re-layouts: 16 us -> none  [the longest x1 10 us: on_device(): picked = flat_back[buffer_row].reshape(token_rows, top_count, width)]
    all_to_all x2 -> x0, starting transfers between devices: 12.2 us -> none  [the longest x1 7.31 us: on_device(): lax.all_to_all(outgoing, 'ep', split_axis=0, concat_axis=0, tiled=True)]
    all_gather x3 -> x0, waiting for transfers between devices: 11.7 us -> none  [the longest x1 11.7 us: on_device(): lax.all_gather(expert_up, 'tp', axis=2, tiled=True)]
    reshape x1 -> x0, local copies, waits for them, and re-layouts: 9.09 us -> none  [on_device(): picked = flat_back[buffer_row].reshape(token_rows, top_count, width)]
  transfers between devices with their start and end apart: 5 -> 0, of which waited for: 3 -> 0; matrix products, arithmetic and copies ran while one was open for 3% -> 0% of each run, Pallas kernels for 0% -> 0%
where the time goes in v1:
time: 209 us
  Pallas kernels  173 us (83%)
  blocking collectives  32.3 us (15%)
  local copies, waits for them, and re-layouts  3.35 us (2%)
    pallas_call x1, Pallas kernels, gathered_plan(): pl.pallas_call(functools.partial(exchange_kernel, line), out_shape=jax.Sh...  173 us
    all_gather x1, blocking collectives, gathered_plan(): everyone = lax.all_gather(weights.T, 'ep').reshape(line, 2, groups, rows)  32.3 us

profile of v1, /device:TPU:0, one launch (start us, length us, event | category | flops | bytes accessed | tf_op | source)
XLA Modules:
  0.0 209.2 jit_solution(5672447507066600585)
XLA Ops:
  0.0 0.7 select_reduce_fusion
  0.7 32.3 %all-gather = f32[64,256]{1,0:T(8,128)S(1)} all-gather(f32[8,256]{1,0:T(8,128)S(1)} %bitcast.14), channel_id=2, replica_groups=mesh['grp'=2,'ep'=8,'tp'=2] {'ep'}, dimensions={0}, use_global_device_ids=true | all-gather | bytes 73728 | tf_op jit(solution)/shard_map/all_gather | solution.py:379
  33.1 1.0 copy.20.wcol
  34.1 172.7 %shard_map.100 = bf16[256,2048]{1,0:T(8,128)(2,1)} custom-call(bf16[256,2048]{1,0:T(8,128)(2,1)} %tok.1, f32[1,2048]{1,0:T(1,128)} %bitcast.15, f32[4,256,2]{2,1,0:T(8,128)} %copy.20.wcol, bf16[2048,256]{1,0:T(8,128)(2,1)} %bitcast.10, bf16[2048,256]{1,0:T(8,128)(2,1)} %bitcast.11, bf16[256,2048]{1,0:T(8,128)(2,1)} %bitcast.12, bf16[2048,512]{1,0:T(8,128)(2,1)} %sg.1, ...), custom_call_target="tpu_custom_call" | custom-call | tf_op jit(solution)/shard_map/pallas_call | solution.py:388
  206.8 2.3 %copy.26 = bf16[256,2048]{1,0:T(8,128)(2,1)} copy(bf16[256,2048]{1,0:T(8,128)(2,1)} %shard_map.100) | data formatting | bytes 2097152
  (3 shorter events, 0.0 us)

commit v2 on v1

--- a/solution.py
+++ b/solution.py
@@ -8,13 +8,13 @@
 from jax.sharding import PartitionSpec as P
 
 MESH = pl.DeviceIdType.MESH
+halves = 2
 
 
 def exchange_kernel(
-    line,
     tok,
     gain,
-    wcol,
+    gate_rows,
     eg,
     eu,
     ed,
@@ -23,6 +23,7 @@
     sd,
     out,
     gathered,
+    gate_of,
     G,
     U,
     D,
@@ -37,6 +38,8 @@
     loc_sem,
     ag_send,
     ag_recv,
+    agw_send,
+    agw_recv,
     w_send,
     w_recv,
     rs_send,
@@ -45,7 +48,7 @@
     rows, width = tok.shape
     half = eg.shape[1]
     shared_width = sg.shape[1]
-    last = line - 1
+    last = gathered.shape[0] - 1
     ep = lax.axis_index("ep")
     z, y = ep // 2, ep % 2
     c = lax.axis_index("tp")
@@ -75,6 +78,7 @@
         pltpu.make_async_copy(eg, G.at[0], loc_sem.at[4]),
         pltpu.make_async_copy(eu, U.at[0], loc_sem.at[5]),
         pltpu.make_async_copy(ed, D.at[pl.ds(0, half)], loc_sem.at[6]),
+        pltpu.make_async_copy(gate_rows, gate_of.at[z], loc_sem.at[7]),
     ]
     for copy in locals_:
         copy.start()
@@ -98,24 +102,32 @@
             device_id_type=MESH,
         )
 
-    def ag_copy(way, step):
+    def ag_copies(way, step):
         block = z - step if way == 0 else z + step
-        src = tok if step == 0 else gathered.at[block]
         peer = to_next if way == 0 else to_prev
-        return remote(
-            src, gathered.at[block], ag_send.at[way, step], ag_recv.at[way, step], peer
-        )
+        return [
+            remote(src if step == 0 else dst.at[block], dst.at[block], a, b, peer)
+            for src, dst, a, b in (
+                (gate_rows, gate_of, agw_send.at[way, step], agw_recv.at[way, step]),
+                (tok, gathered, ag_send.at[way, step], ag_recv.at[way, step]),
+            )
+        ]
 
     def ag_sends(way, step):
         if way == 0:
             return jnp.logical_and(z - step >= 0, z < last)
         return jnp.logical_and(z + step <= last, z > 0)
 
-    def ag_arrival(way, step):
+    def ag_arrivals(way, step):
         block = z - 1 - step if way == 0 else z + 1 + step
-        slot = gathered.at[block]
         peer = to_next if way == 0 else to_prev
-        return remote(slot, slot, ag_send.at[way, step], ag_recv.at[way, step], peer)
+        return [
+            remote(dst.at[block], dst.at[block], a, b, peer)
+            for dst, a, b in (
+                (gate_of, agw_send.at[way, step], agw_recv.at[way, step]),
+                (gathered, ag_send.at[way, step], ag_recv.at[way, step]),
+            )
+        ]
 
     def ag_arrives(way, step):
         return z - 1 - step >= 0 if way == 0 else z + 1 + step <= last
@@ -125,14 +137,16 @@
 
             @pl.when(ag_sends(way, step))
             def _():
-                ag_copy(way, step).start()
+                for copy in ag_copies(way, step):
+                    copy.start()
 
     def ag_wait(step):
         for way in range(2):
 
             @pl.when(ag_arrives(way, step))
             def _():
-                ag_arrival(way, step).wait_recv()
+                for copy in ag_arrivals(way, step):
+                    copy.wait_recv()
 
     def piece(k, unit, part):
         if k == 2:
@@ -198,12 +212,15 @@
 
     def routed(block, fn):
         normalise(block)
+        columns = jnp.transpose(gate_of[block])
+        named = lax.broadcasted_iota(jnp.int32, columns.shape, 1)
 
         @pl.loop(0, 4)
         def _(u):
             a = jnp.dot(xn[...], G[u], preferred_element_type=jnp.float32)
             b = jnp.dot(xn[...], U[u], preferred_element_type=jnp.float32)
-            w = jnp.where(u < 2, wcol[block, :, 0:1], wcol[block, :, 1:2])
+            expert = 2 * z + (y + u // 2) % 2
+            w = jnp.sum(jnp.where(named == expert, columns, 0.0), axis=1, keepdims=True)
             hid[:, pl.ds(pl.multiple_of(u * half, half), half)] = (act(a, b) * w).astype(
                 jnp.bfloat16
             )
@@ -218,6 +235,7 @@
         )
 
     locals_[0].wait()
+    locals_[7].wait()
     normalise(z)
     for copy in locals_[1:4]:
         copy.wait()
@@ -248,110 +266,119 @@
     pass_on(0)
     pass_on(1)
     ag_wait(0)
-    if last > 1:
-        ag_start(1)
+    ag_start(1)
     pass_over(0)
     pass_on(2)
+    ag_wait(1)
+    ag_start(2)
     pass_over(1)
     pass_over(2)
-    for copy in locals_[4:]:
+    for copy in locals_[4:7]:
         copy.wait()
     for kind in (0, 3, 4):
         for k in range(3):
             w_arrival(kind, k).wait_recv()
 
+    near, side = z // 2, z % 2
+    dest = (2 - near, last * (1 - near), z + 1 - 2 * side)
+    ways = (near, near, side)
+    piece_rows = rows // halves
+
+    def part_of(h):
+        return pl.ds(h * piece_rows, piece_rows)
+
+    def rs_copy(i, h):
+        peer = {"ep": ep + 2 - 4 * ways[i]}
+        return remote(
+            stage.at[i, part_of(h)],
+            land.at[ways[i], dest[i], part_of(h)],
+            rs_send.at[i, h],
+            rs_recv.at[ways[i], dest[i], h],
+            peer,
+        )
+
+    def rs_arrival(way, block, h):
+        slot = land.at[way, block, part_of(h)]
+        return remote(slot, slot, rs_send.at[0, h], rs_recv.at[way, block, h], to_pair)
+
+    def over_rows(h, fn):
+        @pl.loop(0, piece_rows // tile)
+        def _(i):
+            fn(pl.ds(pl.multiple_of(h * piece_rows + i * tile, tile), tile))
+
+    def partial(i):
+        def store(cols, value):
+            stage[i, :, cols] = value.astype(jnp.bfloat16)
+
+        routed(dest[i], store)
+
+    def send_first(i):
+        @pl.when(jnp.logical_not(between))
+        def _():
+            for h in range(halves):
+                rs_copy(i, h).start()
+
+    def send_sum(i):
+        @pl.when(between)
+        def _():
+            for h in range(halves):
+                rs_arrival(ways[i], dest[i], h).wait_recv()
+
+                def add(part):
+                    stage[i, part, :] = (
+                        stage[i, part, :].astype(jnp.float32)
+                        + land[ways[i], dest[i], part, :].astype(jnp.float32)
+                    ).astype(jnp.bfloat16)
+
+                over_rows(h, add)
+                rs_copy(i, h).start()
+
+    partial(0)
+    send_first(0)
+    ag_wait(2)
+    partial(1)
+    send_first(1)
+    send_sum(0)
+    partial(2)
+    send_first(2)
+    send_sum(1)
+    send_sum(2)
+
     def add_own(cols, value):
         acc[:, cols] += value
 
     routed(z, add_own)
 
-    def rs_sends(way, t):
-        return jnp.logical_and(z <= t, z < last) if way == 0 else jnp.logical_and(
-            last - z <= t, z > 0
-        )
-
-    def partial(t):
+    for h in range(halves):
         for way in range(2):
 
-            @pl.when(rs_sends(way, t))
+            @pl.when(z > 0 if way == 0 else z < last)
             def _():
-                block = last - t + z if way == 0 else z - last + t
-
-                def store(cols, value):
-                    stage[way, t, :, cols] = value.astype(jnp.bfloat16)
-
-                routed(block, store)
-
-    def rs_copy(way, t):
-        peer = to_next if way == 0 else to_prev
-        return remote(
-            stage.at[way, t], land.at[way, t], rs_send.at[way, t], rs_recv.at[way, t], peer
-        )
-
-    def over_rows(fn):
-        @pl.loop(0, rows // tile)
-        def _(i):
-            fn(pl.ds(pl.multiple_of(i * tile, tile), tile))
-
-    for t in reversed(range(last)):
-        step = last - 1 - t
-        if step > 0:
-            ag_wait(step)
-            if step + 1 < last:
-                ag_start(step + 1)
-        partial(t)
-
-    for t in range(last):
-        for way in range(2):
-
-            @pl.when(rs_sends(way, t))
-            def _():
-                if t > 0:
-                    inner = z > 0 if way == 0 else z < last
-
-                    @pl.when(inner)
-                    def _():
-                        rs_copy(way, t - 1).wait_recv()
-
-                        def add(part):
-                            stage[way, t, part, :] = (
-                                stage[way, t, part, :].astype(jnp.float32)
-                                + land[way, t - 1, part, :].astype(jnp.float32)
-                            ).astype(jnp.bfloat16)
-
-                        over_rows(add)
-
-                rs_copy(way, t).start()
-
-    for way in range(2):
-
-        @pl.when(z > 0 if way == 0 else z < last)
-        def _():
-            rs_copy(way, last - 1).wait_recv()
-
-            def add(part):
-                acc[part, :] += land[way, last - 1, part, :].astype(jnp.float32)
-
-            over_rows(add)
-
-    def finish(part):
-        out[part, :] = acc[part, :].astype(jnp.bfloat16)
-
-    over_rows(finish)
+                rs_arrival(way, z, h).wait_recv()
+
+                def add(part):
+                    acc[part, :] += land[way, z, part, :].astype(jnp.float32)
+
+                over_rows(h, add)
+
+        def finish(part):
+            out[part, :] = acc[part, :].astype(jnp.bfloat16)
+
+        over_rows(h, finish)
 
     for kind in range(5):
         for k in range(3):
             w_copy(kind, k).wait_send()
+    for i in range(3):
+        for h in range(halves):
+            rs_copy(i, h).wait_send()
     for step in range(last):
         for way in range(2):
 
             @pl.when(ag_sends(way, step))
             def _():
-                ag_copy(way, step).wait_send()
-
-            @pl.when(rs_sends(way, step))
-            def _():
-                rs_copy(way, step).wait_send()
+                for copy in ag_copies(way, step):
+                    copy.wait_send()
 
 
 def gathered_plan(
@@ -371,27 +398,23 @@
     line = groups // 2
     half = expert_gate.shape[2]
     shared_width = shared_gate.shape[1]
-    ep = lax.axis_index("ep")
     own = jnp.arange(groups, dtype=jnp.int32)
     weights = jnp.sum(
         jnp.where(routes[:, :, None] == own[None, None, :], gates[:, :, None], 0.0), axis=1
     )
-    everyone = lax.all_gather(weights.T, "ep").reshape(line, 2, groups, rows)
-    mine = lax.dynamic_index_in_dim(everyone, ep % 2, 1, keepdims=False)
-    first = lax.dynamic_index_in_dim(mine, ep, 1, keepdims=False)
-    second = lax.dynamic_index_in_dim(mine, ep // 2 * 2 + 1 - ep % 2, 1, keepdims=False)
-    wcol = jnp.stack([first, second], axis=2)
+    gate_rows = jnp.pad(weights.T, ((0, -groups % 8), (0, 0)))
     any_spec = pl.BlockSpec(memory_space=pl.ANY)
     vmem_spec = pl.BlockSpec(memory_space=pltpu.VMEM)
     bf16 = jnp.bfloat16
     steps = line - 1
     return pl.pallas_call(
-        functools.partial(exchange_kernel, line),
+        exchange_kernel,
         out_shape=jax.ShapeDtypeStruct((rows, width), bf16),
-        in_specs=[any_spec, vmem_spec, vmem_spec] + [any_spec] * 6,
+        in_specs=[any_spec, vmem_spec] + [any_spec] * 7,
         out_specs=vmem_spec,
         scratch_shapes=[
             pltpu.VMEM((line, rows, width), bf16),
+            pltpu.VMEM((line,) + gate_rows.shape, jnp.float32),
             pltpu.VMEM((4, width, half), bf16),
             pltpu.VMEM((4, width, half), bf16),
             pltpu.VMEM((4 * half, width), bf16),
@@ -401,15 +424,17 @@
             pltpu.VMEM((rows, width), bf16),
             pltpu.VMEM((rows, max(4 * half, shared_width)), bf16),
             pltpu.VMEM((rows, width), jnp.float32),
-            pltpu.VMEM((2, steps, rows, width), bf16),
-            pltpu.VMEM((2, steps, rows, width), bf16),
-            pltpu.SemaphoreType.DMA((7,)),
+            pltpu.VMEM((steps, rows, width), bf16),
+            pltpu.VMEM((2, line, rows, width), bf16),
+            pltpu.SemaphoreType.DMA((8,)),
+            pltpu.SemaphoreType.DMA((2, steps)),
+            pltpu.SemaphoreType.DMA((2, steps)),
             pltpu.SemaphoreType.DMA((2, steps)),
             pltpu.SemaphoreType.DMA((2, steps)),
             pltpu.SemaphoreType.DMA((5, 3)),
             pltpu.SemaphoreType.DMA((5, 3)),
-            pltpu.SemaphoreType.DMA((2, steps)),
-            pltpu.SemaphoreType.DMA((2, steps)),
+            pltpu.SemaphoreType.DMA((steps, halves)),
+            pltpu.SemaphoreType.DMA((2, line, halves)),
         ],
         compiler_params=pltpu.CompilerParams(
             collective_id=0, has_side_effects=True, vmem_limit_bytes=56 * 1024 * 1024
@@ -417,7 +442,7 @@
     )(
         tokens,
         norm_gain.reshape(1, width),
-        wcol,
+        gate_rows,
         expert_gate[0],
         expert_up[0],
         expert_down[0],
@@ -490,8 +515,8 @@
 
 def on_device(*args):
     experts = args[4].shape[0] * lax.axis_size("ep")
-    paired = lax.axis_size("grp") == 2 and lax.axis_size("tp") == 2
-    if paired and args[4].shape[0] == 1 and experts % 2 == 0 and experts <= 4 * args[2].shape[1]:
+    paired = lax.axis_size("grp") == 2 and lax.axis_size("tp") == 2 and args[4].shape[0] == 1
+    if paired and experts == 2 * 4 and experts <= 4 * args[2].shape[1]:
         return gathered_plan(*args)
     return routed_plan(*args)
 

time: 209 us -> 139 us (0.67)
  Pallas kernels: 173 us -> 135 us
  blocking collectives: 32.3 us -> 0 us
    pallas_call x1, Pallas kernels: 173 us -> 135 us  [gathered_plan(): pl.pallas_call(exchange_kernel, out_shape=jax.ShapeDtypeStruct((rows, wid...]
    all_gather x1 -> x0, blocking collectives: 32.3 us -> none  [gathered_plan(): everyone = lax.all_gather(weights.T, 'ep').reshape(line, 2, groups, rows)]
where the time goes in v2:
time: 139 us; the launch traced here: 138 us
  Pallas kernels  135 us (97%)
  local copies, waits for them, and re-layouts  2.3 us (2%)
    pallas_call x1, Pallas kernels, gathered_plan(): pl.pallas_call(exchange_kernel, out_shape=jax.ShapeDtypeStruct((rows, wid...  135 us

profile of v2, /device:TPU:0, one launch (start us, length us, event | category | flops | bytes accessed | tf_op | source)
XLA Modules:
  0.0 138.2 jit_solution(2418147921604871308)
XLA Ops:
  0.0 1.3 select_reduce_fusion
  1.3 134.5 %shard_map.100 = bf16[256,2048]{1,0:T(8,128)(2,1)} custom-call(bf16[256,2048]{1,0:T(8,128)(2,1)} %tok.1, f32[1,2048]{1,0:T(1,128)} %bitcast.9, f32[8,256]{1,0:T(8,128)} %bitcast.8, bf16[2048,256]{1,0:T(8,128)(2,1)} %bitcast.5, bf16[2048,256]{1,0:T(8,128)(2,1)} %bitcast.6, bf16[256,2048]{1,0:T(8,128)(2,1)} %bitcast.7, bf16[2048,512]{1,0:T(8,128)(2,1)} %sg.1, ...), custom_call_target="tpu_custom_call" | custom-call | tf_op jit(solution)/shard_map/pallas_call | solution.py:410
  135.9 2.3 %copy.14 = bf16[256,2048]{1,0:T(8,128)(2,1)} copy(bf16[256,2048]{1,0:T(8,128)(2,1)} %shard_map.100) | data formatting | bytes 2097152

commit v3 on v2

--- a/solution.py
+++ b/solution.py
@@ -8,7 +8,7 @@
 from jax.sharding import PartitionSpec as P
 
 MESH = pl.DeviceIdType.MESH
-halves = 2
+pieces = 4
 
 
 def exchange_kernel(
@@ -148,46 +148,44 @@
                 for copy in ag_arrivals(way, step):
                     copy.wait_recv()
 
-    def piece(k, unit, part):
-        if k == 2:
-            if part is None:
-                return D.at[pl.ds(unit * half, half)]
-            n = half // 2
-            return D.at[pl.ds(pl.multiple_of(unit * half + part * n, n), n)]
-        whole = (G, U)[k].at[unit]
-        if part is None:
-            return whole
-        n = width // 2
-        return whole.at[pl.ds(pl.multiple_of(part * n, n), n)]
-
     own = (eg, eu, ed)
 
-    def own_part(k):
-        n = own[k].shape[0] // 2
-        return own[k].at[pl.ds(pl.multiple_of(g * n, n), n)]
+    def cut(ref, base, count, part, parts):
+        n = count // parts
+        return ref.at[pl.ds(pl.multiple_of(base + part * n, n), n)]
+
+    def slot(k, unit, part, parts):
+        if k // 2 == 2:
+            return cut(D, unit * half, half, part, parts)
+        return cut((G, U)[k // 2].at[unit], 0, width, part, parts)
+
+    def owned(k, part, parts):
+        ref = own[k // 2]
+        return cut(ref, 0, ref.shape[0], part, parts)
 
     def w_copy(kind, k):
         sems = (w_send.at[kind, k], w_recv.at[kind, k])
+        mine, theirs = 2 * g + k % 2, 2 * (1 - g) + k % 2
         if kind == 0:
-            return remote(own[k], piece(k, 1, None), *sems, to_core)
+            return remote(owned(k, k % 2, 2), slot(k, 1, k % 2, 2), *sems, to_core)
         if kind == 1:
-            return remote(own_part(k), piece(k, 2, g), *sems, to_pair)
+            return remote(owned(k, mine, 4), slot(k, 2, mine, 4), *sems, to_pair)
         if kind == 2:
-            return remote(piece(k, 2, g), piece(k, 2, g), *sems, to_grp)
+            return remote(slot(k, 2, mine, 4), slot(k, 2, mine, 4), *sems, to_grp)
         if kind == 3:
-            return remote(piece(k, 2, g), piece(k, 3, g), *sems, to_core)
-        return remote(piece(k, 2, 1 - g), piece(k, 3, 1 - g), *sems, to_core)
+            return remote(slot(k, 2, mine, 4), slot(k, 3, mine, 4), *sems, to_core)
+        return remote(slot(k, 2, theirs, 4), slot(k, 3, theirs, 4), *sems, to_core)
 
     def w_arrival(kind, k):
         if kind != 2:
             return w_copy(kind, k)
-        slot = piece(k, 2, 1 - g)
-        return remote(slot, slot, w_send.at[kind, k], w_recv.at[kind, k], to_grp)
+        place = slot(k, 2, 2 * (1 - g) + k % 2, 4)
+        return remote(place, place, w_send.at[kind, k], w_recv.at[kind, k], to_grp)
 
     ag_start(0)
-    for k in range(3):
+    for k in range(6):
         w_copy(1, k).start()
-    for k in range(3):
+    for k in range(6):
         w_copy(0, k).start()
 
     tile = 32
@@ -265,24 +263,30 @@
 
     pass_on(0)
     pass_on(1)
+    pass_over(0)
+    pass_on(2)
+    pass_over(1)
+    pass_on(3)
     ag_wait(0)
     ag_start(1)
-    pass_over(0)
-    pass_on(2)
-    ag_wait(1)
-    ag_start(2)
-    pass_over(1)
     pass_over(2)
+    pass_on(4)
+    pass_over(3)
+    pass_on(5)
+    pass_over(4)
+    pass_over(5)
     for copy in locals_[4:7]:
         copy.wait()
     for kind in (0, 3, 4):
-        for k in range(3):
+        for k in range(6):
             w_arrival(kind, k).wait_recv()
+    ag_wait(1)
+    ag_start(2)
 
     near, side = z // 2, z % 2
     dest = (2 - near, last * (1 - near), z + 1 - 2 * side)
     ways = (near, near, side)
-    piece_rows = rows // halves
+    piece_rows = rows // pieces
 
     def part_of(h):
         return pl.ds(h * piece_rows, piece_rows)
@@ -315,13 +319,13 @@
     def send_first(i):
         @pl.when(jnp.logical_not(between))
         def _():
-            for h in range(halves):
+            for h in range(pieces):
                 rs_copy(i, h).start()
 
     def send_sum(i):
         @pl.when(between)
         def _():
-            for h in range(halves):
+            for h in range(pieces):
                 rs_arrival(ways[i], dest[i], h).wait_recv()
 
                 def add(part):
@@ -349,7 +353,7 @@
 
     routed(z, add_own)
 
-    for h in range(halves):
+    for h in range(pieces):
         for way in range(2):
 
             @pl.when(z > 0 if way == 0 else z < last)
@@ -367,10 +371,10 @@
         over_rows(h, finish)
 
     for kind in range(5):
-        for k in range(3):
+        for k in range(6):
             w_copy(kind, k).wait_send()
     for i in range(3):
-        for h in range(halves):
+        for h in range(pieces):
             rs_copy(i, h).wait_send()
     for step in range(last):
         for way in range(2):
@@ -431,10 +435,10 @@
             pltpu.SemaphoreType.DMA((2, steps)),
             pltpu.SemaphoreType.DMA((2, steps)),
             pltpu.SemaphoreType.DMA((2, steps)),
-            pltpu.SemaphoreType.DMA((5, 3)),
-            pltpu.SemaphoreType.DMA((5, 3)),
-            pltpu.SemaphoreType.DMA((steps, halves)),
-            pltpu.SemaphoreType.DMA((2, line, halves)),
+            pltpu.SemaphoreType.DMA((5, 6)),
+            pltpu.SemaphoreType.DMA((5, 6)),
+            pltpu.SemaphoreType.DMA((steps, pieces)),
+            pltpu.SemaphoreType.DMA((2, line, pieces)),
         ],
         compiler_params=pltpu.CompilerParams(
             collective_id=0, has_side_effects=True, vmem_limit_bytes=56 * 1024 * 1024

time: 139 us -> 131 us (0.942)
  Pallas kernels: 135 us -> 127 us
    pallas_call x1, Pallas kernels: 135 us -> 127 us  [gathered_plan(): pl.pallas_call(exchange_kernel, out_shape=jax.ShapeDtypeStruct((rows, wid...]
where the time goes in v3:
time: 131 us; the launch traced here: 130 us
  Pallas kernels  127 us (97%)
  local copies, waits for them, and re-layouts  2.3 us (2%)
  other arithmetic  1.31 us (1%)
    pallas_call x1, Pallas kernels, gathered_plan(): pl.pallas_call(exchange_kernel, out_shape=jax.ShapeDtypeStruct((rows, wid...  127 us

profile of v3, /device:TPU:0, one launch (start us, length us, event | category | flops | bytes accessed | tf_op | source)
XLA Modules:
  0.0 130.1 jit_solution(4626093474650664185)
XLA Ops:
  0.0 1.3 %select_reduce_fusion = f32[256,8]{0,1:T(8,128)} fusion(f32[256,3]{0,1:T(4,128)} %param.13, s32[256,3]{0,1:T(4,128)} %param.12), kind=kLoop, calls=%fused_computation | loop fusion | flops 16384 | bytes 14336 | tf_op jit(solution)/shard_map/reduce_sum | solution.py:406
  1.3 126.5 %shard_map.100 = bf16[256,2048]{1,0:T(8,128)(2,1)} custom-call(bf16[256,2048]{1,0:T(8,128)(2,1)} %tok.1, f32[1,2048]{1,0:T(1,128)} %bitcast.9, f32[8,256]{1,0:T(8,128)} %bitcast.8, bf16[2048,256]{1,0:T(8,128)(2,1)} %bitcast.5, bf16[2048,256]{1,0:T(8,128)(2,1)} %bitcast.6, bf16[256,2048]{1,0:T(8,128)(2,1)} %bitcast.7, bf16[2048,512]{1,0:T(8,128)(2,1)} %sg.1, ...), custom_call_target="tpu_custom_call" | custom-call | tf_op jit(solution)/shard_map/pallas_call | solution.py:414
  127.8 2.3 %copy.14 = bf16[256,2048]{1,0:T(8,128)(2,1)} copy(bf16[256,2048]{1,0:T(8,128)(2,1)} %shard_map.100) | data formatting | bytes 2097152
